TPU v7x, 32 devices: a whole 2x2x4 slice. The times are simulated.
32 devices in a mesh: rep: 2 (over x), fs: 8 (over z, y), tp: 2 (over core).
Axes of the slice: x: 2, y: 2, z: 4, core: 2. Of those that a mesh axis runs over, the one named last changes fastest.
Arguments:
- pre_gate: bfloat16 [12288, 4096], P(('rep', 'fs'), 'tp'), may hold values from -6 to 6
- pre_linear: bfloat16 [12288, 4096], P(('rep', 'fs'), 'tp'), may hold values from -6 to 6
- taps_gate: float32 [3, 4096], P(None, 'tp'), may hold values from -3.5 to 3.5
- taps_linear: float32 [3, 4096], P(None, 'tp'), may hold values from -3.5 to 3.5
- bias_gate: float32 [4096], P('tp'), may hold values from -3 to 3
- bias_linear: float32 [4096], P('tp'), may hold values from -3 to 3
- down_weight: bfloat16 [4096, 2048], P('tp', 'fs'), may hold values from -0.09375 to 0.09375
- out_grad: bfloat16 [12288, 2048], P(('rep', 'fs')), may hold values from -8 to 8
Outputs:
- grad_gate: bfloat16 [12288, 4096], P(('rep', 'fs'), 'tp')
- grad_linear: bfloat16 [12288, 4096], P(('rep', 'fs'), 'tp')
- grad_taps_gate: float32 [3, 4096], P(None, 'tp')
- grad_taps_linear: float32 [3, 4096], P(None, 'tp')
- grad_bias_gate: float32 [4096], P('tp')
- grad_bias_linear: float32 [4096], P('tp')
- grad_down: float32 [4096, 2048], P('tp', 'fs')
- row_norms: float32 [4096], P('tp')
All inputs are finite; a program needn't handle non-finite values.
Results may differ from a plain program's by a relative error of at most 0.0031.
Values may be sent and summed in bfloat16 or wider, within the bound.
No kernel may reach another device: no remote copies, remote signals or barrier semaphores. Data moves between devices by JAX's collectives and lax.ppermute only.
A program may use at most 128 MiB of HBM per device.

v0:
```python
import jax
import jax.numpy as jnp
from jax import lax
from jax.sharding import PartitionSpec as P


def convolve(values, taps, bias):
    length = values.shape[0]
    padded = jnp.pad(values, ((2, 0), (0, 0)))
    return (
        taps[0] * padded[0:length]
        + taps[1] * padded[1 : length + 1]
        + taps[2] * padded[2 : length + 2]
        + bias
    )


def convolve_back(grads, taps):
    length = grads.shape[0]
    padded = jnp.pad(grads, ((0, 2), (0, 0)))
    return (
        taps[0] * padded[2 : length + 2]
        + taps[1] * padded[1 : length + 1]
        + taps[2] * padded[0:length]
    )


def tap_grads(grads, values):
    length = values.shape[0]
    padded = jnp.pad(values, ((2, 0), (0, 0)))
    return jnp.stack([jnp.sum(grads * padded[j : j + length], axis=0) for j in range(3)])


def local(
    pre_gate, pre_linear, taps_gate, taps_linear, bias_gate, bias_linear, down_weight, out_grad
):
    gate_in = pre_gate.astype(jnp.float32)
    linear_in = pre_linear.astype(jnp.float32)
    gate_pre = convolve(gate_in, taps_gate, bias_gate)
    linear_pre = convolve(linear_in, taps_linear, bias_linear)
    sigma = jax.nn.sigmoid(gate_pre)
    silu_val = gate_pre * sigma
    hidden = (silu_val * linear_pre).astype(jnp.bfloat16)
    columns = out_grad
    grad_hidden = lax.dot_general(
        columns,
        lax.all_gather(down_weight, "fs", axis=1, tiled=True),
        (((1,), (1,)), ((), ())),
        preferred_element_type=jnp.float32,
    )
    grad_gate_pre = grad_hidden * linear_pre * sigma * (1.0 + gate_pre * (1.0 - sigma))
    grad_linear_pre = grad_hidden * silu_val
    grad_gate = convolve_back(grad_gate_pre, taps_gate).astype(jnp.bfloat16)
    grad_linear = convolve_back(grad_linear_pre, taps_linear).astype(jnp.bfloat16)
    conv_parts = (
        tap_grads(grad_gate_pre, gate_in),
        tap_grads(grad_linear_pre, linear_in),
        jnp.sum(grad_gate_pre, axis=0),
        jnp.sum(grad_linear_pre, axis=0),
    )
    grad_taps_gate, grad_taps_linear, grad_bias_gate, grad_bias_linear = lax.psum(
        (conv_parts[0], conv_parts[1], conv_parts[2], conv_parts[3]), ("rep", "fs")
    )
    columns = out_grad
    partial_grad = lax.psum_scatter(
        lax.dot_general(
            columns, hidden, (((0,), (0,)), ((), ())), preferred_element_type=jnp.float32
        ),
        "fs",
        scatter_dimension=0,
        tiled=True,
    )
    summed = lax.psum(partial_grad, "rep")
    grad_down = summed.T
    row_norms = lax.psum(jnp.sum(grad_down * grad_down, axis=1), "fs")
    return (
        grad_gate,
        grad_linear,
        grad_taps_gate,
        grad_taps_linear,
        grad_bias_gate,
        grad_bias_linear,
        grad_down,
        row_norms,
    )


def solution(mesh):
    in_specs = (
        P(("rep", "fs"), "tp"),
        P(("rep", "fs"), "tp"),
        P(None, "tp"),
        P(None, "tp"),
        P("tp"),
        P("tp"),
        P("tp", "fs"),
        P(("rep", "fs"), None),
    )
    out_specs = (
        P(("rep", "fs"), "tp"),
        P(("rep", "fs"), "tp"),
        P(None, "tp"),
        P(None, "tp"),
        P("tp"),
        P("tp"),
        P("tp", "fs"),
        P("tp"),
    )
    return jax.shard_map(local, mesh=mesh, in_specs=in_specs, out_specs=out_specs, check_vma=False)
```

profile of v0, /device:TPU:0, one launch (start us, length us, event | category | flops | bytes accessed | tf_op | source)
XLA Modules:
  0.0 668.1 jit_solution(7865275278848254621)
XLA Ops:
  7.2 0.0 copy-start
  7.2 0.0 all-gather.2.cloned.1.call-start
  7.2 0.7 all-gather.2.cloned.1.call-update
  7.9 0.0 reduce-scatter.2.cloned.1.call-start
  8.0 0.0 copy-start.3
  8.0 5.6 convert_element_type.24
  13.5 0.0 copy-done.3
  13.5 0.0 copy-start.4
  13.5 0.0 copy-start.5
  13.5 0.0 copy-start.7
  13.5 3.4 convert_element_type.23
  17.0 0.0 copy-done.4
  17.0 0.0 copy-done.5
  17.0 120.7 %all-gather.2.cloned.1.call-done = bf16[2048,2048]{1,0:T(8,128)(2,1)} async-done(((bf16[2048,256]{1,0:T(8,128)(2,1)}), bf16[2048,2048]{1,0:T(8,128)(2,1)}) %all-gather.2.cloned.1.call-update) | async-done | bytes 8388624 | tf_op jit(solution)/shard_map/all_gather | solution.py:47
  137.7 0.0 copy-done
  137.7 0.0 copy-done.7
  137.7 0.0 copy-start.1
  137.7 0.0 copy-start.2
  137.7 0.0 copy-start.6
  137.8 25.9 %fusion.4 = (f32[2048]{0:T(1024)}, f32[2048]{0:T(1024)S(1)}, f32[2048]{0:T(1024)S(1)}, f32[2048]{0:T(1024)S(1)}, f32[768,2048]{1,0:T(8,128)}, /*index=5*/f32[768,2048]{1,0:T(8,128)}, f32[768,2048]{1,0:T(8,128)}) fusion(bf16[768,2048]{1,0:T(8,128)(2,1)} %param.9, f32[768,2048]{1,0:T(8,128)} %convert_element_type.23, f32[2048]{0:T(1024)S(1)} %copy-done.7, ...), kind=kOutput, calls=%fused_computation.24 | convolution fusion | flops 6472327168 | bytes 46202880 | tf_op jit(solution)/shard_map/dot_general | solution.py:45
  163.7 0.0 copy-done.1
  163.7 0.0 copy-done.2
  163.7 0.0 copy-done.6
  163.7 19.0 %fusion.5 = (f32[2048]{0:T(1024)}, f32[2048]{0:T(1024)S(1)}, f32[2048]{0:T(1024)S(1)}, f32[2048]{0:T(1024)S(1)}, f32[768,2048]{1,0:T(8,128)}, /*index=5*/f32[768,2048]{1,0:T(8,128)}, bf16[768,2048]{1,0:T(8,128)(2,1)}) fusion(bf16[768,2048]{1,0:T(8,128)(2,1)} %param.8, f32[768,2048]{1,0:T(8,128)S(1)} %copy-done.1, f32[768,2048]{1,0:T(8,128)} %get-tuple-element.25, ...), kind=kLoop, calls=%fused_computation.25 | loop fusion | flops 45604864 | bytes 50397184 | tf_op jit(solution)/shard_map/reduce_sum | solution.py:58
  182.7 15.2 %convolution_bitcast_fusion = f32[2048,2048]{0,1:T(8,128)} fusion(bf16[768,2048]{1,0:T(8,128)(2,1)S(1)} %copy-done, f32[768,2048]{1,0:T(8,128)} %get-tuple-element.27, f32[768,2048]{1,0:T(8,128)} %get-tuple-element.25), kind=kOutput, calls=%fused_computation | convolution fusion | flops 6451888128 | bytes 32505856 | tf_op jit(solution)/shard_map/dot_general | solution.py:66
  197.8 0.0 reduce-scatter.2.cloned.1.call-update
  197.9 0.0 all-reduce.8.cloned.1.call-start
  197.9 278.5 %reduce-scatter.2.cloned.1.call-done = f32[256,2048]{0,1:T(8,128)} async-done(((f32[2048,2048]{0,1:T(8,128)}), f32[256,2048]{0,1:T(8,128)}) %reduce-scatter.2.cloned.1.call-update) | async-done | bytes 2097168 | tf_op jit(solution)/shard_map/reduce_scatter | solution.py:65
  476.4 0.0 all-reduce.8.cloned.1.call-update
  476.5 0.0 all-reduce.10.cloned.1.call-start
  476.5 0.7 pad_maximum_fusion
  477.2 9.6 %add_convert_fusion.1 = bf16[768,2048]{1,0:T(8,128)(2,1)} fusion(f32[768,2048]{1,0:T(8,128)} %get-tuple-element.26, f32[2048]{0:T(1024)S(1)} %bitcast.28, f32[2048]{0:T(1024)S(1)} %bitcast.30, f32[2048]{0:T(1024)S(1)} %bitcast.26), kind=kLoop, calls=%fused_computation.9 | loop fusion | flops 9437184 | bytes 9461760 | tf_op jit(solution)/shard_map/convert_element_type | solution.py:53
  486.8 0.0 all-reduce.10.cloned.1.call-update
  486.8 54.0 %all-reduce.8.cloned.1.call-done = f32[2048,256]{1,0:T(8,128)} async-done(((f32[2048,256]{1,0:T(8,128)}), f32[2048,256]{1,0:T(8,128)}) %all-reduce.8.cloned.1.call-update) | async-done | bytes 2097168 | tf_op jit(solution)/shard_map/psum | solution.py:73
  540.8 1.9 multiply_reduce_fusion.6
  542.8 22.3 %psum.47 = f32[2048]{0:T(1024)} all-reduce(f32[2048]{0:T(1024)S(1)} %multiply_reduce_fusion.6), channel_id=1, replica_groups=mesh['rep'=2,'fs'=8,'tp'=2] {'fs'}, use_global_device_ids=true, to_apply=%region_15.16 | all-reduce | flops 2048 | bytes 16384 | tf_op jit(solution)/shard_map/psum | solution.py:75
  565.1 88.1 %all-reduce.10.cloned.1.call-done = (f32[3,2048]{1,0:T(4,128)}, f32[3,2048]{1,0:T(4,128)}, f32[2048]{0:T(1024)}, f32[2048]{0:T(1024)}) async-done(((f32[3,2048]{1,0:T(4,128)}, f32[3,2048]{1,0:T(4,128)}, f32[2048]{0:T(1024)}, f32[2048]{0:T(1024)}), (f32[3,2048]{1,0:T(4,128)}, f32[3,2048]{1,0:T(4,128)}, f32[2048]{0:T(1024)}, f32[2048]{0:T(1024)})) %all-reduce.10.cloned.1.call-update) | async-done | bytes 65552 | tf_op jit(solution)/shard_map/psum | solution.py:61
  653.2 1.4 copy.21
  654.6 1.4 copy.22
  655.9 1.3 copy.23
  657.2 1.3 copy.24
  658.5 3.0 copy.25
  (2 shorter events, 0.0 us)
Async XLA Ops:
  7.2 130.6 %copy-start = (bf16[768,2048]{1,0:T(8,128)(2,1)S(1)}, bf16[768,2048]{1,0:T(8,128)(2,1)}, u32[]{:S(2)}) copy-start(bf16[768,2048]{1,0:T(8,128)(2,1)} %param.15) | copy-start | bytes 9437188
  7.2 130.5 %all-gather.2.cloned.1.call-start = ((), (), s32[]{:S(2)}) async-start(), calls=%async_computation.1 | async-start | bytes 9437184 | tf_op jit(solution)/shard_map/all_gather | solution.py:47
  7.9 468.5 %reduce-scatter.2.cloned.1.call-start = ((), (), s32[]{:S(2)}) async-start(), calls=%async_computation.2 | async-start | bytes 18874368 | tf_op jit(solution)/shard_map/reduce_scatter | solution.py:65
  8.0 5.6 copy-start.3
  13.5 3.4 copy-start.4
  13.5 3.5 copy-start.5
  13.5 124.2 %copy-start.7 = (f32[2048]{0:T(1024)S(1)}, f32[2048]{0:T(1024)}, u32[]{:S(2)}) copy-start(f32[2048]{0:T(1024)} %param.12) | copy-start | bytes 24580
  137.7 25.9 %copy-start.1 = (f32[768,2048]{1,0:T(8,128)S(1)}, f32[768,2048]{1,0:T(8,128)}, u32[]{:S(2)}) copy-start(f32[768,2048]{1,0:T(8,128)} %convert_element_type.24) | copy-start | bytes 18874372
  137.7 25.9 %copy-start.2 = (f32[768,2048]{1,0:T(8,128)S(1)}, f32[768,2048]{1,0:T(8,128)}, u32[]{:S(2)}) copy-start(f32[768,2048]{1,0:T(8,128)} %convert_element_type.23) | copy-start | bytes 18874372
  137.7 25.9 %copy-start.6 = (f32[2048]{0:T(1024)S(1)}, f32[2048]{0:T(1024)}, u32[]{:S(2)}) copy-start(f32[2048]{0:T(1024)} %param.13) | copy-start | bytes 24580
  197.9 343.0 %all-reduce.8.cloned.1.call-start = ((), (), s32[]{:S(2)}) async-start(), calls=%async_computation.3 | async-start | bytes 4194304 | tf_op jit(solution)/shard_map/psum | solution.py:73
  476.5 176.7 %all-reduce.10.cloned.1.call-start = ((), (), s32[]{:S(2)}) async-start(), calls=%async_computation.4 | async-start | bytes 163840 | tf_op jit(solution)/shard_map/psum | solution.py:61
Sparse Core Ops, SparseCore 0:
  10.0 127.6 all-gather.1
  198.0 278.3 reduce-scatter.1
  478.7 62.0 all-reduce.7
  547.2 105.9 all-reduce.9
where the time goes:
time: 669 us; the launch traced here: 668 us
  waiting for transfers between devices  542 us (81%)
  matrix products  41.1 us (6%)
  other arithmetic  40.2 us (6%)
  blocking collectives  22.3 us (3%)
  between operations  13.8 us (2%)
  local copies, waits for them, and re-layouts  8.47 us (1%)
    reduce_scatter x1, waiting for transfers between devices, local(): lax.psum_scatter(lax.dot_general(columns, hidden, (((0,), (0,)), ((), ())...  279 us
    all_gather x1, waiting for transfers between devices, local(): lax.all_gather(down_weight, 'fs', axis=1, tiled=True)  121 us
    psum x1, waiting for transfers between devices, local(): lax.psum((conv_parts[0], conv_parts[1], conv_parts[2], conv_parts[3]), ('...  88.1 us
    psum x1, waiting for transfers between devices, local(): summed = lax.psum(partial_grad, 'rep')  54 us
    dot_general x1, matrix products, local(): lax.dot_general(columns, lax.all_gather(down_weight, 'fs', axis=1, tiled=...  25.9 us
    psum x1, blocking collectives, local(): row_norms = lax.psum(jnp.sum(grad_down * grad_down, axis=1), 'fs')  22.3 us
    reduce_sum x1, other arithmetic, local(): jnp.sum(grad_gate_pre, axis=0)  19 us
    dot_general x1, matrix products, local(): lax.dot_general(columns, hidden, (((0,), (0,)), ((), ())), preferred_elem...  15.2 us
  transfers between devices with their start and end apart: 4, of which 4 were waited for; matrix products, arithmetic and copies ran while one was open for 3% of the time, Pallas kernels for 0%

commit v1 on v0

--- a/solution.py
+++ b/solution.py
@@ -44,7 +44,7 @@
     columns = out_grad
     grad_hidden = lax.dot_general(
         columns,
-        lax.all_gather(down_weight, "fs", axis=1, tiled=True),
+        jnp.concatenate(lax.all_gather(down_weight, "fs"), axis=1),
         (((1,), (1,)), ((), ())),
         preferred_element_type=jnp.float32,
     )

time: 669 us -> 689 us (1.030)
  local copies, waits for them, and re-layouts: 8.47 us -> 19.9 us
  other arithmetic: 40.2 us -> 48.9 us
    reshape x0 -> x1, local copies, waits for them, and re-layouts: none -> 11.4 us  [local(): jnp.concatenate(lax.all_gather(down_weight, 'fs'), axis=1)]
    reduce_sum x1, other arithmetic: 19 us -> 27.6 us  [local(): jnp.sum(grad_gate_pre, axis=0)]
where the time goes in v1:
time: 689 us; the launch traced here: 688 us
  waiting for transfers between devices  542 us (79%)
  other arithmetic  48.9 us (7%)
  matrix products  41.6 us (6%)
  blocking collectives  22.3 us (3%)
  local copies, waits for them, and re-layouts  19.9 us (3%)
  between operations  13.8 us (2%)
    reduce_scatter x1, waiting for transfers between devices, local(): lax.psum_scatter(lax.dot_general(columns, hidden, (((0,), (0,)), ((), ())...  279 us
    all_gather x1, waiting for transfers between devices, local(): lax.all_gather(down_weight, 'fs')  120 us
    psum x1, waiting for transfers between devices, local(): lax.psum((conv_parts[0], conv_parts[1], conv_parts[2], conv_parts[3]), ('...  88.1 us
    psum x1, waiting for transfers between devices, local(): summed = lax.psum(partial_grad, 'rep')  54 us
    dot_general x1, matrix products, local(): lax.dot_general(columns, jnp.concatenate(lax.all_gather(down_weight, 'fs'...  28 us
    reduce_sum x1, other arithmetic, local(): jnp.sum(grad_gate_pre, axis=0)  27.6 us
    psum x1, blocking collectives, local(): row_norms = lax.psum(jnp.sum(grad_down * grad_down, axis=1), 'fs')  22.3 us
  transfers between devices with their start and end apart: 4, of which 4 were waited for; matrix products, arithmetic and copies ran while one was open for 3% of the time, Pallas kernels for 0%

profile of v1, /device:TPU:0, one launch (start us, length us, event | category | flops | bytes accessed | tf_op | source)
XLA Modules:
  0.0 688.3 jit_solution(17979869887643094355)
XLA Ops:
  7.2 0.0 copy-start
  7.2 0.0 all-gather.3.cloned.1.call-start
  7.2 0.7 all-gather.3.cloned.1.call-update
  7.9 0.0 reduce-scatter.2.cloned.1.call-start
  8.0 0.0 copy-start.3
  8.0 5.6 convert_element_type.24
  13.5 0.0 copy-done.3
  13.5 0.0 copy-start.4
  13.5 0.0 copy-start.5
  13.5 3.5 convert_element_type.23
  17.0 0.0 copy-done.4
  17.0 0.0 copy-done.5
  17.1 120.3 %all-gather.3.cloned.1.call-done = bf16[16384,256]{1,0:T(8,128)(2,1)} async-done(((bf16[2048,256]{1,0:T(8,128)(2,1)}), bf16[16384,256]{1,0:T(8,128)(2,1)}) %all-gather.3.cloned.1.call-update) | async-done | bytes 8388624 | tf_op jit(solution)/shard_map/all_gather | solution.py:47
  137.3 0.0 copy-start.7
  137.4 11.4 %copy.16 = bf16[2048,8,256]{0,2,1:T(8,128)(2,1)} copy(bf16[2048,8,256]{2,0,1:T(8,128)(2,1)} %bitcast.22) | data formatting | bytes 16777216 | tf_op jit(solution)/shard_map/reshape | solution.py:47
  148.8 0.0 copy-done
  148.8 0.0 copy-done.7
  148.8 0.0 copy-start.1
  148.8 0.0 copy-start.6
  148.8 28.0 %fusion.4 = (f32[2048]{0:T(1024)}, f32[2048]{0:T(1024)S(1)}, f32[2048]{0:T(1024)S(1)}, f32[2048]{0:T(1024)S(1)}, f32[768,2048]{1,0:T(8,128)}, /*index=5*/f32[768,2048]{1,0:T(8,128)}, f32[768,2048]{1,0:T(8,128)}) fusion(bf16[768,2048]{1,0:T(8,128)(2,1)} %param.9, f32[768,2048]{1,0:T(8,128)} %convert_element_type.23, f32[2048]{0:T(1024)S(1)} %copy-done.7, ...), kind=kOutput, calls=%fused_computation.24 | convolution fusion | flops 6472327168 | bytes 46202880 | tf_op jit(solution)/shard_map/dot_general | solution.py:45
  176.8 0.0 copy-done.1
  176.8 0.0 copy-done.6
  176.9 0.0 copy-start.2
  176.9 27.6 %fusion.5 = (f32[2048]{0:T(1024)}, f32[2048]{0:T(1024)S(1)}, f32[2048]{0:T(1024)S(1)}, f32[2048]{0:T(1024)S(1)}, f32[768,2048]{1,0:T(8,128)}, /*index=5*/f32[768,2048]{1,0:T(8,128)}, bf16[768,2048]{1,0:T(8,128)(2,1)}) fusion(bf16[768,2048]{1,0:T(8,128)(2,1)S(1)} %copy-done.1, f32[768,2048]{1,0:T(8,128)} %convert_element_type.24, ...), kind=kLoop, calls=%fused_computation.25 | loop fusion | flops 45604864 | bytes 50397184 | tf_op jit(solution)/shard_map/reduce_sum | solution.py:58
  204.5 0.0 copy-done.2
  204.5 13.6 %convolution_bitcast_fusion = f32[2048,2048]{0,1:T(8,128)} fusion(bf16[768,2048]{1,0:T(8,128)(2,1)S(1)} %copy-done, f32[768,2048]{1,0:T(8,128)} %get-tuple-element.27, f32[768,2048]{1,0:T(8,128)S(1)} %copy-done.2), kind=kOutput, calls=%fused_computation | convolution fusion | flops 6451888128 | bytes 32505856 | tf_op jit(solution)/shard_map/dot_general | solution.py:66
  218.1 0.0 reduce-scatter.2.cloned.1.call-update
  218.1 0.0 all-reduce.8.cloned.1.call-start
  218.1 278.5 %reduce-scatter.2.cloned.1.call-done = f32[256,2048]{0,1:T(8,128)} async-done(((f32[2048,2048]{0,1:T(8,128)}), f32[256,2048]{0,1:T(8,128)}) %reduce-scatter.2.cloned.1.call-update) | async-done | bytes 2097168 | tf_op jit(solution)/shard_map/reduce_scatter | solution.py:65
  496.7 0.0 all-reduce.8.cloned.1.call-update
  496.7 0.0 all-reduce.10.cloned.1.call-start
  496.7 0.7 pad_maximum_fusion
  497.4 9.6 %add_convert_fusion.1 = bf16[768,2048]{1,0:T(8,128)(2,1)} fusion(f32[768,2048]{1,0:T(8,128)} %get-tuple-element.26, f32[2048]{0:T(1024)S(1)} %bitcast.34, f32[2048]{0:T(1024)S(1)} %bitcast.36, f32[2048]{0:T(1024)S(1)} %bitcast.32), kind=kLoop, calls=%fused_computation.9 | loop fusion | flops 9437184 | bytes 9461760 | tf_op jit(solution)/shard_map/convert_element_type | solution.py:53
  507.0 0.0 all-reduce.10.cloned.1.call-update
  507.0 54.0 %all-reduce.8.cloned.1.call-done = f32[2048,256]{1,0:T(8,128)} async-done(((f32[2048,256]{1,0:T(8,128)}), f32[2048,256]{1,0:T(8,128)}) %all-reduce.8.cloned.1.call-update) | async-done | bytes 2097168 | tf_op jit(solution)/shard_map/psum | solution.py:73
  561.1 1.9 multiply_reduce_fusion.6
  563.0 22.3 %psum.47 = f32[2048]{0:T(1024)} all-reduce(f32[2048]{0:T(1024)S(1)} %multiply_reduce_fusion.6), channel_id=1, replica_groups=mesh['rep'=2,'fs'=8,'tp'=2] {'fs'}, use_global_device_ids=true, to_apply=%region_15.16 | all-reduce | flops 2048 | bytes 16384 | tf_op jit(solution)/shard_map/psum | solution.py:75
  585.3 88.1 %all-reduce.10.cloned.1.call-done = (f32[3,2048]{1,0:T(4,128)}, f32[3,2048]{1,0:T(4,128)}, f32[2048]{0:T(1024)}, f32[2048]{0:T(1024)}) async-done(((f32[3,2048]{1,0:T(4,128)}, f32[3,2048]{1,0:T(4,128)}, f32[2048]{0:T(1024)}, f32[2048]{0:T(1024)}), (f32[3,2048]{1,0:T(4,128)}, f32[3,2048]{1,0:T(4,128)}, f32[2048]{0:T(1024)}, f32[2048]{0:T(1024)})) %all-reduce.10.cloned.1.call-update) | async-done | bytes 65552 | tf_op jit(solution)/shard_map/psum | solution.py:61
  673.4 1.4 copy.22
  674.8 1.4 copy.23
  676.2 1.3 copy.24
  677.5 1.3 copy.25
  678.8 3.0 copy.26
  (2 shorter events, 0.0 us)
Async XLA Ops:
  7.2 141.6 %copy-start = (bf16[768,2048]{1,0:T(8,128)(2,1)S(1)}, bf16[768,2048]{1,0:T(8,128)(2,1)}, u32[]{:S(2)}) copy-start(bf16[768,2048]{1,0:T(8,128)(2,1)} %param.15) | copy-start | bytes 9437188
  7.2 130.2 %all-gather.3.cloned.1.call-start = ((), (), s32[]{:S(2)}) async-start(), calls=%async_computation.3 | async-start | bytes 9437184 | tf_op jit(solution)/shard_map/all_gather | solution.py:47
  7.9 488.7 %reduce-scatter.2.cloned.1.call-start = ((), (), s32[]{:S(2)}) async-start(), calls=%async_computation.1 | async-start | bytes 18874368 | tf_op jit(solution)/shard_map/reduce_scatter | solution.py:65
  8.0 5.6 copy-start.3
  13.5 3.5 copy-start.4
  13.5 3.5 copy-start.5
  137.3 11.5 %copy-start.7 = (f32[2048]{0:T(1024)S(1)}, f32[2048]{0:T(1024)}, u32[]{:S(2)}) copy-start(f32[2048]{0:T(1024)} %param.12) | copy-start | bytes 24580
  148.8 28.0 %copy-start.1 = (bf16[768,2048]{1,0:T(8,128)(2,1)S(1)}, bf16[768,2048]{1,0:T(8,128)(2,1)}, u32[]{:S(2)}) copy-start(bf16[768,2048]{1,0:T(8,128)(2,1)} %param.8) | copy-start | bytes 9437188
  148.8 28.0 %copy-start.6 = (f32[2048]{0:T(1024)S(1)}, f32[2048]{0:T(1024)}, u32[]{:S(2)}) copy-start(f32[2048]{0:T(1024)} %param.13) | copy-start | bytes 24580
  176.9 27.6 %copy-start.2 = (f32[768,2048]{1,0:T(8,128)S(1)}, f32[768,2048]{1,0:T(8,128)}, u32[]{:S(2)}) copy-start(f32[768,2048]{1,0:T(8,128)} %get-tuple-element.25) | copy-start | bytes 18874372
  218.1 343.0 %all-reduce.8.cloned.1.call-start = ((), (), s32[]{:S(2)}) async-start(), calls=%async_computation.2 | async-start | bytes 4194304 | tf_op jit(solution)/shard_map/psum | solution.py:73
  496.7 176.7 %all-reduce.10.cloned.1.call-start = ((), (), s32[]{:S(2)}) async-start(), calls=%async_computation.4 | async-start | bytes 163840 | tf_op jit(solution)/shard_map/psum | solution.py:61
Sparse Core Ops, SparseCore 0:
  10.1 127.1 all-gather.2
  218.2 278.3 reduce-scatter.1
  498.9 62.0 all-reduce.7
  567.4 105.9 all-reduce.9
